TPU v7x, 128 devices: a whole 4x4x4 slice. The times are simulated.
128 devices in a mesh: sp: 16 (over z, y), dp: 8 (over x, core).
Axes of the slice: x: 4, y: 4, z: 4, core: 2. Of those that a mesh axis runs over, the one named last changes fastest.
Arguments:
- inputs: bfloat16 [8, 3072, 2048], P('dp', 'sp'), may hold values from -6 to 6
- in_gain: float32 [2048], replicated, may hold values from 0.1 to 1.9
- w_query: bfloat16 [2048, 1024], P('dp', 'sp'), may hold values from -0.125 to 0.125
- w_key: bfloat16 [2048, 256], P('dp', 'sp'), may hold values from -0.375 to 0.375
- w_value: bfloat16 [2048, 256], P('dp', 'sp'), may hold values from -0.125 to 0.125
- key_bias: float32 [8, 3072, 16], P('dp', None, 'sp'), may hold values from -20 to 0
- out_gain: float32 [1024], replicated, may hold values from 0.1 to 1.9
- w_out: bfloat16 [1024, 2048], P('sp', 'dp'), may hold values from -0.1875 to 0.1875
Outputs:
- mixed: bfloat16 [8, 3072, 2048], P('dp', 'sp')
All inputs are finite; a program needn't handle non-finite values.
Results may differ from a plain program's by a relative error of at most 0.012.
The roundings to bfloat16 on the way count: a program that leaves them out, or rounds other values in their place, can miss the bound.
Values may be sent and summed in bfloat16 or wider, within the bound.
A program may use at most 128 MiB of HBM per device.

v0:
```python
import jax
import jax.numpy as jnp
from jax import lax
from jax.sharding import PartitionSpec as P

HEAD_DIM = 64
norm_eps = 1e-06


def rows_first(arrays, axis, dims):
    turned = [jnp.moveaxis(a, dim, 0) for a, dim in zip(arrays, dims)]
    both = jnp.concatenate([t.reshape(len(t), -1) for t in turned], axis=1)
    whole, at, finished = (lax.all_gather(both, axis, axis=0, tiled=True), 0, [])
    for t, dim in zip(turned, dims):
        slab = whole[:, at : at + t[0].size].reshape(-1, *t.shape[1:])
        finished.append(jnp.moveaxis(slab, 0, dim))
        at += t[0].size
    return tuple(finished)


def sent_together(arrays, axis, split_dim, concat_dim, along):
    ends, at = ([], 0)
    for a in arrays[:-1]:
        at += a.shape[along]
        ends.append(at)
    both = jnp.concatenate(arrays, axis=along)
    return tuple(
        jnp.split(
            lax.all_to_all(both, axis, split_axis=split_dim, concat_axis=concat_dim, tiled=True),
            ends,
            axis=along,
        )
    )


def body(inputs, in_gain, w_query, w_key, w_value, key_bias, out_gain, w_out):
    width_sp = lax.axis_size("sp")
    own_index = lax.axis_index("sp")
    wide = inputs[0].astype(jnp.float32)
    normed_rows = (
        wide * lax.rsqrt(jnp.mean(wide * wide, axis=-1, keepdims=True) + norm_eps) * in_gain
    ).astype(jnp.bfloat16)
    local_rows = normed_rows.shape[0]
    w_query, w_key, w_value, w_out = rows_first(
        (w_query, w_key, w_value, w_out), "dp", (0, 0, 0, 1)
    )
    w_key, w_value = rows_first((w_key, w_value), "sp", (1, 1))
    keys = jnp.dot(normed_rows, w_key, preferred_element_type=jnp.float32).astype(jnp.bfloat16)
    values = jnp.dot(normed_rows, w_value, preferred_element_type=jnp.float32).astype(jnp.bfloat16)
    queries = jnp.dot(
        normed_rows,
        lax.all_gather(w_query, "sp", axis=1, tiled=True),
        preferred_element_type=jnp.float32,
    ).astype(jnp.bfloat16)
    heads_here = key_bias.shape[2]
    kv_heads = keys.shape[1] // HEAD_DIM
    spread = width_sp // kv_heads
    query_slots = queries.reshape(local_rows, width_sp, heads_here * HEAD_DIM)
    key_copies = jnp.repeat(keys.reshape(local_rows, kv_heads, HEAD_DIM), spread, axis=1)
    value_copies = jnp.repeat(values.reshape(local_rows, kv_heads, HEAD_DIM), spread, axis=1)
    query_all, key_all, value_all = sent_together(
        (query_slots, key_copies, value_copies), "sp", 1, 0, 2
    )
    keys_head = key_all[:, 0, :]
    values_head = value_all[:, 0, :]
    length_all = query_all.shape[0]
    bias_here = key_bias[0].T
    block = min(512, length_all)
    pieces = []
    for index in range(length_all // block):
        start = index * block
        end = start + block
        logits = jnp.einsum(
            "thd,sd->hts", query_all[start:end], keys_head[:end], preferred_element_type=jnp.float32
        )
        logits = logits * HEAD_DIM ** (-0.5) + bias_here[:, None, :end]
        rows = start + jnp.arange(block, dtype=jnp.int32)[:, None]
        columns = jnp.arange(end, dtype=jnp.int32)[None, :]
        strict = (columns < rows)[None, :, :]
        log_keep = jnp.where(strict, jax.nn.log_sigmoid(-logits), jnp.float32(0.0))
        log_rest = lax.cumsum(log_keep, axis=2, reverse=True) - log_keep
        sticks = jnp.where(
            strict, jnp.exp(jax.nn.log_sigmoid(logits) + log_rest), jnp.float32(0.0)
        ).astype(jnp.bfloat16)
        pieces.append(
            jnp.einsum("hts,sd->thd", sticks, values_head[:end], preferred_element_type=jnp.float32)
        )
    attended = jnp.concatenate(pieces, axis=0)
    gains = lax.dynamic_slice_in_dim(
        out_gain, own_index * heads_here * HEAD_DIM, heads_here * HEAD_DIM, 0
    )
    scaled = attended * lax.rsqrt(jnp.mean(attended * attended, axis=-1, keepdims=True) + norm_eps)
    head_out = (scaled * gains.reshape(heads_here, HEAD_DIM)).astype(jnp.bfloat16)
    returned = lax.all_to_all(head_out, "sp", split_axis=0, concat_axis=1, tiled=True)
    returned = returned.reshape(local_rows, width_sp * heads_here * HEAD_DIM)
    mixed = jnp.dot(
        returned,
        lax.all_gather(w_out, "sp", axis=0, tiled=True),
        preferred_element_type=jnp.float32,
    )
    return mixed.astype(jnp.bfloat16)[None]


def solution(mesh):
    placed = (
        P("dp", "sp", None),
        P(),
        P("dp", "sp"),
        P("dp", "sp"),
        P("dp", "sp"),
        P("dp", None, "sp"),
        P(),
        P("sp", "dp"),
    )
    return jax.shard_map(
        body, mesh=mesh, in_specs=placed, out_specs=P("dp", "sp", None), check_vma=False
    )
```

profile of v0, /device:TPU:0, one launch (start us, length us, event | category | flops | bytes accessed | tf_op | source)
XLA Modules:
  0.0 349.7 jit_solution(17781443614021492482)
XLA Ops:
  7.4 13.7 %all_gather.12 = bf16[2048,160]{0,1:T(8,128)(2,1)S(1)} all-gather(bf16[256,160]{0,1:T(8,128)(2,1)S(1)} %pad_maximum_fusion.2), channel_id=1, replica_groups=mesh['sp'=16,'dp'=8] {'dp'}, dimensions={0}, use_global_device_ids=true | all-gather | bytes 737280 | tf_op jit(solution)/shard_map/all_gather | solution.py:13
  23.0 45.8 %all-gather.6.cloned.1.call-done = bf16[256,4096]{1,0:T(8,128)(2,1)} async-done(((bf16[16,4096]{1,0:T(8,128)(2,1)}), bf16[256,4096]{1,0:T(8,128)(2,1)}) %all-gather.6.cloned.1.call-update) | async-done | bytes 2097168 | tf_op jit(solution)/shard_map/all_gather | solution.py:13
  68.8 1.9 convolution_convert_fusion.2
  71.4 50.3 %all-gather.4.cloned.1.call-done = bf16[2048,1024]{0,1:T(8,128)(2,1)} async-done(((bf16[2048,64]{0,1:T(8,128)(2,1)}), bf16[2048,1024]{0,1:T(8,128)(2,1)}) %all-gather.4.cloned.1.call-update) | async-done | bytes 4194320 | tf_op jit(solution)/shard_map/all_gather | solution.py:52
  121.7 3.7 %convolution_convert_fusion.1 = bf16[192,1024]{1,0:T(8,128)(2,1)S(1)} fusion(bf16[2048,1024]{0,1:T(8,128)(2,1)} %all-gather.4.cloned.1.call-done, bf16[1,192,2048]{2,1,0:T(8,128)(2,1)S(1)} %copy-done.4, f32[2048]{0:T(1024)S(1)} %copy-done.7, f32[192]{0:T(256)S(1)} %add_rsqrt_fusion.1), kind=kOutput, calls=%fused_computation.128 | convolution fusion | flops 807075840 | bytes 5382912 | tf_op jit(solution)/shard_map/dot_general | solution.py:50
  127.2 5.3 %all-to-all-start = ((bf16[192,16,192]{0,2,1:T(8,128)(2,1)}), bf16[192,16,192]{0,2,1:T(8,128)(2,1)S(1)}, u32[]{:S(2)}, u32[]{:S(2)}) async-start(bf16[192,16,192]{0,2,1:T(8,128)(2,1)} %pad_maximum_fusion), calls=%async_computation | async-start | bytes 3145728 | tf_op jit(solution)/shard_map/all_to_all | solution.py:29
  134.2 23.7 %all-to-all-done = bf16[192,16,192]{0,2,1:T(8,128)(2,1)S(1)} async-done(((bf16[192,16,192]{0,2,1:T(8,128)(2,1)}), bf16[192,16,192]{0,2,1:T(8,128)(2,1)S(1)}, u32[]{:S(2)}, u32[]{:S(2)}) %all-to-all-start) | async-done | bytes 1179680 | tf_op jit(solution)/shard_map/all_to_all | solution.py:29
  158.7 1.7 all_to_all.27
  162.1 4.8 %fusion.121 = f32[1,512,4,128]{1,2,3,0:T(4,128)S(1)} fusion(f32[1,512,4,128]{1,3,2,0:T(8,128)S(1)} %bitcast.409), kind=kOutput, calls=%fused_computation.155 | output fusion | flops 33292288 | bytes 2097152 | tf_op jit(solution)/shard_map/reduce-window
  168.2 2.9 fusion.66
  171.0 5.2 %fusion.74 = f32[1,512,8,128]{1,2,3,0:T(8,128)S(1)} fusion(f32[1,512,8,128]{1,3,2,0:T(8,128)S(1)} %bitcast.404), kind=kOutput, calls=%fused_computation.113 | output fusion | flops 66584576 | bytes 4194304 | tf_op jit(solution)/shard_map/reduce-window.2
  176.2 2.6 copy.63
  178.8 4.1 %fusion.53 = (f32[1,512,1536]{1,2,0:T(8,128)S(1)}, f32[1,512,1536]{1,2,0:T(8,128)}) fusion(s32[512]{0:T(512)S(1)} %iota_add_fusion.3, f32[1536]{0:T(1024)S(1)} %slice_reduce_fusion.1, bf16[3072,1,192]{0,2,1:T(8,128)(2,1)S(1)} %all_to_all.27), kind=kOutput, calls=%fused_computation.82 | convolution fusion | flops 109314048 | bytes 6563840 | tf_op jit(solution)/shard_map/thd,sd->hts/dot_general | solution.py:73
  182.9 10.1 %fusion.42 = f32[1,512,12,128]{1,2,3,0:T(8,128)S(1)} fusion(f32[1,512,12,128]{1,3,2,0:T(8,128)S(1)} %bitcast.402), kind=kOutput, calls=%fused_computation.69 | output fusion | flops 99876864 | bytes 6291456 | tf_op jit(solution)/shard_map/reduce-window.4
  193.0 1.8 copy.65
  194.9 6.1 %fusion.34 = (f32[1,512,2048]{1,2,0:T(8,128)S(1)}, f32[2048,512]{1,0:T(8,128)}) fusion(f32[2048]{0:T(1024)S(1)} %bitcast.419, s32[512]{0:T(512)S(1)} %iota_add_fusion.2, bf16[3072,1,192]{0,2,1:T(8,128)(2,1)} %copy-done.1), kind=kOutput, calls=%fused_computation.56 | convolution fusion | flops 145752064 | bytes 8726528 | tf_op jit(solution)/shard_map/thd,sd->hts/dot_general | solution.py:73
  201.0 10.3 %fusion.40 = f32[1,512,16,128]{1,2,3,0:T(8,128)S(1)} fusion(f32[1,512,16,128]{1,3,2,0:T(8,128)S(1)} %bitcast.401), kind=kOutput, calls=%fused_computation.67 | output fusion | flops 133169152 | bytes 8388608 | tf_op jit(solution)/shard_map/reduce-window.6
  211.3 4.4 %copy.67 = f32[1,512,16,128]{1,3,2,0:T(8,128)} copy(f32[1,512,16,128]{1,2,3,0:T(8,128)S(1)} %fusion.40) | data formatting | bytes 8388608 | tf_op jit(solution)/shard_map/reduce-window.6
  215.8 7.1 %fusion.22 = (f32[1,512,2560]{1,2,0:T(8,128)S(1)}, f32[2560,512,1]{1,0,2:T(8,128)}) fusion(s32[512]{0:T(512)S(1)} %iota_add_fusion.1, f32[2560]{0:T(1024)S(1)} %slice_reduce_fusion, bf16[3072,1,192]{0,2,1:T(8,128)(2,1)} %copy-done.1), kind=kOutput, calls=%fused_computation.38 | convolution fusion | flops 182190080 | bytes 10891264 | tf_op jit(solution)/shard_map/thd,sd->hts/dot_general | solution.py:73
  222.9 15.6 %fusion.14 = f32[1,512,20,128]{1,2,3,0:T(8,128)S(1)} fusion(f32[1,512,20,128]{1,3,2,0:T(8,128)S(1)} %bitcast.400), kind=kOutput, calls=%fused_computation.27 | output fusion | flops 166461440 | bytes 10485760 | tf_op jit(solution)/shard_map/reduce-window.8
  238.5 5.4 %copy.69 = f32[1,512,20,128]{1,3,2,0:T(8,128)} copy(f32[1,512,20,128]{1,2,3,0:T(8,128)S(1)} %fusion.14) | data formatting | bytes 10485760 | tf_op jit(solution)/shard_map/reduce-window.8
  244.0 8.2 %fusion.6 = (f32[1,512,3072]{1,2,0:T(8,128)S(1)}, f32[3072,512]{1,0:T(8,128)}) fusion(f32[3072]{0:T(1024)S(1)} %bitcast.417, s32[512]{0:T(512)S(1)} %iota_add_fusion, bf16[3072,1,192]{0,2,1:T(8,128)(2,1)} %copy-done.1), kind=kOutput, calls=%fused_computation.14 | convolution fusion | flops 218628096 | bytes 13056000 | tf_op jit(solution)/shard_map/thd,sd->hts/dot_general | solution.py:73
  252.2 15.3 %fusion.12 = f32[1,512,24,128]{1,2,3,0:T(8,128)S(1)} fusion(f32[1,512,24,128]{1,3,2,0:T(8,128)S(1)} %bitcast.398), kind=kOutput, calls=%fused_computation.25 | output fusion | flops 199753728 | bytes 12582912 | tf_op jit(solution)/shard_map/reduce-window.10
  267.5 6.3 %copy.71 = f32[1,512,24,128]{1,3,2,0:T(8,128)} copy(f32[1,512,24,128]{1,2,3,0:T(8,128)S(1)} %fusion.12) | data formatting | bytes 12582912 | tf_op jit(solution)/shard_map/reduce-window.10
  274.0 2.6 fusion.114
  276.7 5.8 %fusion.64 = bf16[1,512,1024]{1,2,0:T(8,128)(2,1)S(1)} fusion(f32[1,512,8,128]{1,3,2,0:T(8,128)} %copy.63, f32[1024,512]{1,0:T(8,128)} %get-tuple-element.12, f32[512,8]{0,1:T(8,128)S(1)} %slice_bitcast_fusion.47, f32[1024]{0:T(1024)S(1)} %bitcast.423, s32[512]{0:T(512)S(1)} %iota_add_fusion.4), kind=kLoop, calls=%fused_computation.98 | loop fusion | flops 12582912 | bytes 5265408 | tf_op jit(solution)/shard_map/convert_element_type | solution.py:84
  282.5 6.4 %fusion.51 = bf16[1,512,1536]{1,2,0:T(8,128)(2,1)S(1)} fusion(f32[1,512,12,128]{1,3,2,0:T(8,128)S(1)} %copy.65, f32[1,512,1536]{1,2,0:T(8,128)} %get-tuple-element.14, f32[512,12]{0,1:T(8,128)S(1)} %slice_bitcast_fusion.45, s32[512]{0:T(512)S(1)} %iota_add_fusion.3), kind=kLoop, calls=%fused_computation.80 | loop fusion | flops 17301504 | bytes 7890944 | tf_op jit(solution)/shard_map/convert_element_type | solution.py:84
  288.9 7.3 %fusion.32 = bf16[1,512,2048]{1,2,0:T(8,128)(2,1)S(1)} fusion(f32[1,512,16,128]{1,3,2,0:T(8,128)S(1)} %copy-done, f32[2048,512]{1,0:T(8,128)S(1)} %copy-done.3, f32[512,16]{0,1:T(8,128)S(1)} %slice_bitcast_fusion.43, f32[2048]{0:T(1024)S(1)} %bitcast.420, s32[512]{0:T(512)S(1)} %iota_add_fusion.2), kind=kLoop, calls=%fused_computation.54 | loop fusion | flops 25165824 | bytes 10528768 | tf_op jit(solution)/shard_map/convert_element_type | solution.py:84
  296.3 9.8 %fusion.20 = bf16[1,512,2560]{1,2,0:T(8,128)(2,1)S(1)} fusion(f32[1,512,20,128]{1,3,2,0:T(8,128)S(1)} %bitcast.395, f32[2560,512,1]{1,0,2:T(8,128)} %get-tuple-element.18, f32[512,20]{0,1:T(8,128)S(1)} %slice_bitcast_fusion.41, s32[512]{0:T(512)S(1)} %iota_add_fusion.1), kind=kLoop, calls=%fused_computation.36 | loop fusion | flops 28835840 | bytes 13150208 | tf_op jit(solution)/shard_map/convert_element_type | solution.py:84
  306.2 10.9 %fusion.4 = bf16[1,512,3072]{1,2,0:T(8,128)(2,1)S(1)} fusion(f32[1,512,24,128]{1,3,2,0:T(8,128)S(1)} %bitcast.393, f32[3072,512]{1,0:T(8,128)S(1)} %bitcast.397, f32[512,24]{0,1:T(8,128)S(1)} %slice_bitcast_fusion.39, f32[3072]{0:T(1024)S(1)} %bitcast.418, s32[512]{0:T(512)S(1)} %iota_add_fusion), kind=kLoop, calls=%fused_computation.12 | loop fusion | flops 37748736 | bytes 15792128 | tf_op jit(solution)/shard_map/convert_element_type | solution.py:84
  322.4 13.3 %all_to_all.33 = bf16[16,2,6144]{2,1,0:T(2,128)(2,1)S(1)} all-to-all(bf16[16,2,6144]{2,1,0:T(2,128)(2,1)S(1)} %reshape.777), channel_id=1, replica_groups=mesh['sp'=16,'dp'=8] {'sp'}, dimensions={0} | all-to-all | bytes 786432 | tf_op jit(solution)/shard_map/all_to_all | solution.py:94
  338.8 4.1 %fusion.59 = bf16[1,192,2048]{2,1,0:T(8,128)(2,1)} fusion(bf16[192,1024]{0,1:T(8,128)(2,1)S(1)} %bitcast.408, bf16[1024,2048]{1,0:T(8,128)(2,1)} %all-gather.8.cloned.1.call-done), kind=kOutput, calls=%fused_computation.93 | convolution fusion | flops 805699584 | bytes 5373952 | tf_op jit(solution)/shard_map/dot_general | solution.py:96
  (100 shorter events, 19.5 us)
Async XLA Ops:
  6.5 16.2 %copy-start.4 = (bf16[1,192,2048]{2,1,0:T(8,128)(2,1)S(1)}, bf16[1,192,2048]{2,1,0:T(8,128)(2,1)}, u32[]{:S(2)}) copy-start(bf16[1,192,2048]{2,1,0:T(8,128)(2,1)} %param.8) | copy-start | bytes 2359300
  6.5 62.3 %copy-start.7 = (f32[2048]{0:T(1024)S(1)}, f32[2048]{0:T(1024)}, u32[]{:S(2)}) copy-start(f32[2048]{0:T(1024)} %param.9) | copy-start | bytes 24580
  6.5 62.2 %all-gather.6.cloned.1.call-start = ((), (), s32[]{:S(2)}) async-start(), calls=%async_computation.3 | async-start | bytes 2228224 | tf_op jit(solution)/shard_map/all_gather | solution.py:13
  21.8 99.9 %all-gather.4.cloned.1.call-start = ((), (), s32[]{:S(2)}) async-start(), calls=%async_computation.2 | async-start | bytes 4456448 | tf_op jit(solution)/shard_map/all_gather | solution.py:52
  68.8 2.0 copy-start.6
  125.8 7.5 %copy-start.5 = (f32[1,3072,1]{1,2,0:T(1,128)S(1)}, f32[1,3072,1]{1,2,0:T(1,128)}, u32[]{:S(2)}) copy-start(f32[1,3072,1]{1,2,0:T(1,128)} %param.13) | copy-start | bytes 36868
  127.2 30.6 %all-to-all-start = ((bf16[192,16,192]{0,2,1:T(8,128)(2,1)}), bf16[192,16,192]{0,2,1:T(8,128)(2,1)S(1)}, u32[]{:S(2)}, u32[]{:S(2)}) async-start(bf16[192,16,192]{0,2,1:T(8,128)(2,1)} %pad_maximum_fusion), calls=%async_computation | async-start | bytes 3145728 | tf_op jit(solution)/shard_map/all_to_all | solution.py:29
  132.5 206.2 %all-gather.8.cloned.1.call-start = ((), (), s32[]{:S(2)}) async-start(), calls=%async_computation.4 | async-start | bytes 4456448 | tf_op jit(solution)/shard_map/all_gather | solution.py:98
  160.4 18.4 %copy-start.1 = (bf16[3072,1,192]{0,2,1:T(8,128)(2,1)}, bf16[3072,1,192]{0,2,1:T(8,128)(2,1)S(1)}, u32[]{:S(2)}) copy-start(bf16[3072,1,192]{0,2,1:T(8,128)(2,1)S(1)} %all_to_all.27) | copy-start | bytes 3538948
  274.0 14.8 %copy-start.3 = (f32[2048,512]{1,0:T(8,128)S(1)}, f32[2048,512]{1,0:T(8,128)}, u32[]{:S(2)}) copy-start(f32[2048,512]{1,0:T(8,128)} %get-tuple-element.16) | copy-start | bytes 12582916
  276.7 19.6 %slice-start.2 = ((s8[5242880]{0:T(1024)(128)(4,1)}), s8[4194304]{0:T(1024)(128)(4,1)S(1)}, s32[]{:S(2)}) async-start(s8[5242880]{0:T(1024)(128)(4,1)} %bitcast.394), calls=%async_computation.7 | async-start | bytes 8388608
  282.4 6.4 %copy-start = (f32[1,512,16,128]{1,3,2,0:T(8,128)S(1)}, f32[1,512,16,128]{1,3,2,0:T(8,128)}, u32[]{:S(2)}) copy-start(f32[1,512,16,128]{1,3,2,0:T(8,128)} %copy.67) | copy-start | bytes 12582916
  282.4 13.8 %slice-start.3 = ((s8[5242880]{0:T(1024)(128)(4,1)}), s8[1048576]{0:T(1024)(128)(4,1)S(1)}, s32[]{:S(2)}) async-start(s8[5242880]{0:T(1024)(128)(4,1)} %bitcast.394), calls=%async_computation.8 | async-start | bytes 2097152
  288.9 17.3 %slice-start = ((s8[6291456]{0:T(1024)(128)(4,1)}), s8[4194304]{0:T(1024)(128)(4,1)S(1)}, s32[]{:S(2)}) async-start(s8[6291456]{0:T(1024)(128)(4,1)} %bitcast.392), calls=%async_computation.5 | async-start | bytes 8388608
  288.9 17.3 %slice-start.4 = ((s8[6291456]{0:T(1024)(128)(4,1)}), s8[2097152]{0:T(1024)(128)(4,1)S(1)}, s32[]{:S(2)}) async-start(s8[6291456]{0:T(1024)(128)(4,1)} %bitcast.396), calls=%async_computation.9 | async-start | bytes 4194304
  296.2 9.9 %slice-start.1 = ((s8[6291456]{0:T(1024)(128)(4,1)}), s8[2097152]{0:T(1024)(128)(4,1)S(1)}, s32[]{:S(2)}) async-start(s8[6291456]{0:T(1024)(128)(4,1)} %bitcast.392), calls=%async_computation.6 | async-start | bytes 4194304
  296.2 9.9 %slice-start.5 = ((s8[6291456]{0:T(1024)(128)(4,1)}), s8[4194304]{0:T(1024)(128)(4,1)S(1)}, s32[]{:S(2)}) async-start(s8[6291456]{0:T(1024)(128)(4,1)} %bitcast.396), calls=%async_computation.10 | async-start | bytes 8388608
  306.2 10.9 %copy-start.2 = (bf16[3072,1,192]{0,2,1:T(8,128)(2,1)S(1)}, bf16[3072,1,192]{0,2,1:T(8,128)(2,1)}, u32[]{:S(2)}) copy-start(bf16[3072,1,192]{0,2,1:T(8,128)(2,1)} %copy-done.1) | copy-start | bytes 3538948
Sparse Core Ops, SparseCore 0:
  21.9 46.8 all-gather.5
  70.9 50.7 all-gather.3
  135.5 54.9 all-gather.7
where the time goes:
time: 353 us; the launch traced here: 350 us
  waiting for transfers between devices  120 us (34%)
  other arithmetic  109 us (31%)
  matrix products  42.7 us (12%)
  local copies, waits for them, and re-layouts  31.2 us (9%)
  blocking collectives  27 us (8%)
  between operations  14 us (4%)
  starting transfers between devices  5.9 us (2%)
    another operation x12, other arithmetic  61.8 us
    all_gather x1, waiting for transfers between devices, body(): lax.all_gather(w_query, 'sp', axis=1, tiled=True)  50.3 us
    all_gather x1, waiting for transfers between devices, rows_first(): lax.all_gather(both, axis, axis=0, tiled=True)  45.8 us
    convert_element_type x6, other arithmetic, body(): sticks = jnp.where(strict, jnp.exp(jax.nn.log_sigmoid(logits) + log_rest)...  42.8 us
    dot_general x6, matrix products, body(): jnp.einsum('thd,sd->hts', query_all[start:end], keys_head[:end], preferre...  29.9 us
    all_to_all x1, waiting for transfers between devices, sent_together(): lax.all_to_all(both, axis, split_axis=split_dim, concat_axis=concat_dim,...  23.7 us
    another operation x18, local copies, waits for them, and re-layouts  21.8 us
    all_gather x1, blocking collectives, rows_first(): lax.all_gather(both, axis, axis=0, tiled=True)  13.7 us
  transfers between devices with their start and end apart: 4, of which 3 were waited for; matrix products, arithmetic and copies ran while one was open for 48% of the time, Pallas kernels for 0%

commit v1 on v0

--- a/solution.py
+++ b/solution.py
@@ -1,3 +1,4 @@
+import functools
 import jax
 import jax.numpy as jnp
 from jax import lax
@@ -5,6 +6,14 @@
 
 HEAD_DIM = 64
 norm_eps = 1e-06
+
+
+def draw_body(inner_x, comm_axis):
+    work_now = jnp.concatenate([inner_x] * lax.axis_size(comm_axis), axis=1)
+    return lax.all_to_all(work_now, axis_name=comm_axis, split_axis=1, concat_axis=1, tiled=True)
+
+
+raise_the_node = functools.partial(draw_body, comm_axis="sp")
 
 
 def rows_first(arrays, axis, dims):
@@ -48,9 +57,7 @@
     keys = jnp.dot(normed_rows, w_key, preferred_element_type=jnp.float32).astype(jnp.bfloat16)
     values = jnp.dot(normed_rows, w_value, preferred_element_type=jnp.float32).astype(jnp.bfloat16)
     queries = jnp.dot(
-        normed_rows,
-        lax.all_gather(w_query, "sp", axis=1, tiled=True),
-        preferred_element_type=jnp.float32,
+        normed_rows, raise_the_node(w_query), preferred_element_type=jnp.float32
     ).astype(jnp.bfloat16)
     heads_here = key_bias.shape[2]
     kv_heads = keys.shape[1] // HEAD_DIM

time: 353 us -> 342 us (0.969)
  waiting for transfers between devices: 120 us -> 99.5 us
  starting transfers between devices: 5.9 us -> 13.4 us
    all_gather x1 -> x0, waiting for transfers between devices: 50.3 us -> none  [body(): lax.all_gather(w_query, 'sp', axis=1, tiled=True)]
    all_gather x1, waiting for transfers between devices: 45.8 us -> 76.7 us  [rows_first(): lax.all_gather(both, axis, axis=0, tiled=True)]
    all_to_all x0 -> x1, starting transfers between devices: none -> 8.23 us  [draw_body(): lax.all_to_all(work_now, axis_name=comm_axis, split_axis=1, concat_axis=1...]
  transfers between devices with their start and end apart: 4 -> 4, of which waited for: 3 -> 2; matrix products, arithmetic and copies ran while one was open for 48% -> 50% of each run, Pallas kernels for 0% -> 0%
where the time goes in v1:
time: 342 us; the launch traced here: 338 us
  other arithmetic  108 us (32%)
  waiting for transfers between devices  99.5 us (29%)
  matrix products  43.7 us (13%)
  local copies, waits for them, and re-layouts  33.4 us (10%)
  blocking collectives  25.7 us (8%)
  between operations  14.6 us (4%)
  starting transfers between devices  13.4 us (4%)
    all_gather x1, waiting for transfers between devices, rows_first(): lax.all_gather(both, axis, axis=0, tiled=True)  76.7 us
    another operation x12, other arithmetic  61.9 us
    convert_element_type x6, other arithmetic, body(): sticks = jnp.where(strict, jnp.exp(jax.nn.log_sigmoid(logits) + log_rest)...  41.3 us
    dot_general x6, matrix products, body(): jnp.einsum('thd,sd->hts', query_all[start:end], keys_head[:end], preferre...  29.9 us
    all_to_all x1, waiting for transfers between devices, sent_together(): lax.all_to_all(both, axis, split_axis=split_dim, concat_axis=concat_dim,...  22.2 us
    another operation x18, local copies, waits for them, and re-layouts  21.8 us
    all_gather x1, blocking collectives, rows_first(): lax.all_gather(both, axis, axis=0, tiled=True)  13.7 us
    all_to_all x1, blocking collectives, body(): lax.all_to_all(head_out, 'sp', split_axis=0, concat_axis=1, tiled=True)  12 us
  transfers between devices with their start and end apart: 4, of which 2 were waited for; matrix products, arithmetic and copies ran while one was open for 50% of the time, Pallas kernels for 0%

profile of v1, /device:TPU:0, one launch (start us, length us, event | category | flops | bytes accessed | tf_op | source)
XLA Modules:
  0.0 337.9 jit_solution(15754657176527293575)
XLA Ops:
  7.4 13.7 %all_gather.9 = bf16[2048,160]{0,1:T(8,128)(2,1)S(1)} all-gather(bf16[256,160]{0,1:T(8,128)(2,1)S(1)} %pad_maximum_fusion.2), channel_id=1, replica_groups=mesh['sp'=16,'dp'=8] {'dp'}, dimensions={0}, use_global_device_ids=true | all-gather | bytes 737280 | tf_op jit(solution)/shard_map/all_gather | solution.py:22
  22.9 2.0 copy-done.3
  24.9 8.2 %all-to-all-start = ((bf16[2048,16,64]{0,2,1:T(8,128)(2,1)}), bf16[2048,16,64]{0,2,1:T(8,128)(2,1)}, u32[]{:S(2)}, u32[]{:S(2)}) async-start(bf16[2048,16,64]{0,2,1:T(8,128)(2,1)} %bitcast.415), calls=%async_computation | async-start | bytes 8388608 | tf_op jit(solution)/shard_map/all_to_all | solution.py:13
  33.4 76.7 %all-gather.3.cloned.1.call-done = bf16[256,4096]{1,0:T(8,128)(2,1)} async-done(((bf16[16,4096]{1,0:T(8,128)(2,1)}), bf16[256,4096]{1,0:T(8,128)(2,1)}) %all-gather.3.cloned.1.call-update) | async-done | bytes 2097168 | tf_op jit(solution)/shard_map/all_gather | solution.py:22
  111.9 1.7 convolution_convert_fusion.3
  113.8 3.7 %convolution_convert_fusion.1 = bf16[192,1024]{1,0:T(8,128)(2,1)S(1)} fusion(bf16[2048,1024]{0,1:T(8,128)(2,1)} %bitcast.4, bf16[1,192,2048]{2,1,0:T(8,128)(2,1)S(1)} %copy-done.5, f32[2048]{0:T(1024)S(1)} %copy-done.7, f32[192]{0:T(256)S(1)} %add_rsqrt_fusion.1), kind=kOutput, calls=%fused_computation.132 | convolution fusion | flops 807075840 | bytes 5382912 | tf_op jit(solution)/shard_map/dot_general | solution.py:59
  119.3 4.9 %all-to-all-start.1 = ((bf16[192,16,192]{0,2,1:T(8,128)(2,1)}), bf16[192,16,192]{0,2,1:T(8,128)(2,1)S(1)}, u32[]{:S(2)}, u32[]{:S(2)}) async-start(bf16[192,16,192]{0,2,1:T(8,128)(2,1)} %pad_maximum_fusion), calls=%async_computation.1 | async-start | bytes 3145728 | tf_op jit(solution)/shard_map/all_to_all | solution.py:38
  125.9 22.2 %all-to-all-done.1 = bf16[192,16,192]{0,2,1:T(8,128)(2,1)S(1)} async-done(((bf16[192,16,192]{0,2,1:T(8,128)(2,1)}), bf16[192,16,192]{0,2,1:T(8,128)(2,1)S(1)}, u32[]{:S(2)}, u32[]{:S(2)}) %all-to-all-start.1) | async-done | bytes 1179680 | tf_op jit(solution)/shard_map/all_to_all | solution.py:38
  152.4 4.8 %fusion.125 = f32[1,512,4,128]{1,2,3,0:T(4,128)S(1)} fusion(f32[1,512,4,128]{1,3,2,0:T(8,128)S(1)} %bitcast.424), kind=kOutput, calls=%fused_computation.159 | output fusion | flops 33292288 | bytes 2097152 | tf_op jit(solution)/shard_map/reduce-window
  158.5 2.9 fusion.66
  161.3 5.4 %fusion.74 = f32[1,512,8,128]{1,2,3,0:T(8,128)S(1)} fusion(f32[1,512,8,128]{1,3,2,0:T(8,128)S(1)} %bitcast.419), kind=kOutput, calls=%fused_computation.113 | output fusion | flops 66584576 | bytes 4194304 | tf_op jit(solution)/shard_map/reduce-window.2
  166.8 2.6 copy.63
  169.4 4.1 %fusion.53 = (f32[1,512,1536]{1,2,0:T(8,128)S(1)}, f32[1,512,1536]{1,2,0:T(8,128)}) fusion(s32[512]{0:T(512)S(1)} %iota_add_fusion.3, f32[1536]{0:T(1024)S(1)} %slice_reduce_fusion.1, bf16[3072,1,192]{0,2,1:T(8,128)(2,1)S(1)} %all_to_all.38), kind=kOutput, calls=%fused_computation.82 | convolution fusion | flops 109314048 | bytes 6563840 | tf_op jit(solution)/shard_map/thd,sd->hts/dot_general | solution.py:80
  173.4 10.1 %fusion.42 = f32[1,512,12,128]{1,2,3,0:T(8,128)S(1)} fusion(f32[1,512,12,128]{1,3,2,0:T(8,128)S(1)} %bitcast.417), kind=kOutput, calls=%fused_computation.69 | output fusion | flops 99876864 | bytes 6291456 | tf_op jit(solution)/shard_map/reduce-window.4
  183.5 1.8 copy.65
  185.5 6.0 %fusion.34 = (f32[1,512,2048]{1,2,0:T(8,128)S(1)}, f32[2048,512]{1,0:T(8,128)}) fusion(f32[2048]{0:T(1024)S(1)} %bitcast.434, s32[512]{0:T(512)S(1)} %iota_add_fusion.2, bf16[3072,1,192]{0,2,1:T(8,128)(2,1)} %copy-done.1), kind=kOutput, calls=%fused_computation.56 | convolution fusion | flops 145752064 | bytes 8726528 | tf_op jit(solution)/shard_map/thd,sd->hts/dot_general | solution.py:80
  191.5 10.2 %fusion.40 = f32[1,512,16,128]{1,2,3,0:T(8,128)S(1)} fusion(f32[1,512,16,128]{1,3,2,0:T(8,128)S(1)} %bitcast.416), kind=kOutput, calls=%fused_computation.67 | output fusion | flops 133169152 | bytes 8388608 | tf_op jit(solution)/shard_map/reduce-window.6
  201.8 4.4 %copy.67 = f32[1,512,16,128]{1,3,2,0:T(8,128)} copy(f32[1,512,16,128]{1,2,3,0:T(8,128)S(1)} %fusion.40) | data formatting | bytes 8388608 | tf_op jit(solution)/shard_map/reduce-window.6
  206.3 7.1 %fusion.22 = (f32[1,512,2560]{1,2,0:T(8,128)S(1)}, f32[2560,512,1]{1,0,2:T(8,128)}) fusion(s32[512]{0:T(512)S(1)} %iota_add_fusion.1, f32[2560]{0:T(1024)S(1)} %slice_reduce_fusion, bf16[3072,1,192]{0,2,1:T(8,128)(2,1)} %copy-done.1), kind=kOutput, calls=%fused_computation.38 | convolution fusion | flops 182190080 | bytes 10891264 | tf_op jit(solution)/shard_map/thd,sd->hts/dot_general | solution.py:80
  213.4 15.5 %fusion.14 = f32[1,512,20,128]{1,2,3,0:T(8,128)S(1)} fusion(f32[1,512,20,128]{1,3,2,0:T(8,128)S(1)} %bitcast.414), kind=kOutput, calls=%fused_computation.27 | output fusion | flops 166461440 | bytes 10485760 | tf_op jit(solution)/shard_map/reduce-window.8
  228.9 5.4 %copy.69 = f32[1,512,20,128]{1,3,2,0:T(8,128)} copy(f32[1,512,20,128]{1,2,3,0:T(8,128)S(1)} %fusion.14) | data formatting | bytes 10485760 | tf_op jit(solution)/shard_map/reduce-window.8
  234.5 8.2 %fusion.6 = (f32[1,512,3072]{1,2,0:T(8,128)S(1)}, f32[3072,512]{1,0:T(8,128)}) fusion(f32[3072]{0:T(1024)S(1)} %bitcast.432, s32[512]{0:T(512)S(1)} %iota_add_fusion, bf16[3072,1,192]{0,2,1:T(8,128)(2,1)} %copy-done.1), kind=kOutput, calls=%fused_computation.14 | convolution fusion | flops 218628096 | bytes 13056000 | tf_op jit(solution)/shard_map/thd,sd->hts/dot_general | solution.py:80
  242.6 15.3 %fusion.12 = f32[1,512,24,128]{1,2,3,0:T(8,128)S(1)} fusion(f32[1,512,24,128]{1,3,2,0:T(8,128)S(1)} %bitcast.410), kind=kOutput, calls=%fused_computation.25 | output fusion | flops 199753728 | bytes 12582912 | tf_op jit(solution)/shard_map/reduce-window.10
  257.9 6.3 %copy.71 = f32[1,512,24,128]{1,3,2,0:T(8,128)} copy(f32[1,512,24,128]{1,2,3,0:T(8,128)S(1)} %fusion.12) | data formatting | bytes 12582912 | tf_op jit(solution)/shard_map/reduce-window.10
  264.5 2.6 fusion.118
  267.1 5.8 %fusion.64 = bf16[1,512,1024]{1,2,0:T(8,128)(2,1)S(1)} fusion(f32[1,512,8,128]{1,3,2,0:T(8,128)} %copy.63, f32[1024,512]{1,0:T(8,128)} %get-tuple-element.12, f32[512,8]{0,1:T(8,128)S(1)} %slice_bitcast_fusion.47, f32[1024]{0:T(1024)S(1)} %bitcast.438, s32[512]{0:T(512)S(1)} %iota_add_fusion.4), kind=kLoop, calls=%fused_computation.98 | loop fusion | flops 12582912 | bytes 5265408 | tf_op jit(solution)/shard_map/convert_element_type | solution.py:91
  272.9 4.9 %fusion.51 = bf16[1,512,1536]{1,2,0:T(8,128)(2,1)S(1)} fusion(f32[1,512,12,128]{1,3,2,0:T(8,128)S(1)} %copy.65, f32[1,512,1536]{1,2,0:T(8,128)S(1)} %copy-done.4, f32[512,12]{0,1:T(8,128)S(1)} %slice_bitcast_fusion.45, s32[512]{0:T(512)S(1)} %iota_add_fusion.3), kind=kLoop, calls=%fused_computation.80 | loop fusion | flops 17301504 | bytes 7890944 | tf_op jit(solution)/shard_map/convert_element_type | solution.py:91
  277.9 8.9 %fusion.32 = bf16[1,512,2048]{1,2,0:T(8,128)(2,1)S(1)} fusion(f32[1,512,16,128]{1,3,2,0:T(8,128)S(1)} %copy-done, f32[2048,512]{1,0:T(8,128)} %get-tuple-element.16, f32[512,16]{0,1:T(8,128)S(1)} %slice_bitcast_fusion.43, f32[2048]{0:T(1024)S(1)} %bitcast.435, s32[512]{0:T(512)S(1)} %iota_add_fusion.2), kind=kLoop, calls=%fused_computation.54 | loop fusion | flops 25165824 | bytes 10528768 | tf_op jit(solution)/shard_map/convert_element_type | solution.py:91
  286.9 8.2 %fusion.20 = bf16[1,512,2560]{1,2,0:T(8,128)(2,1)S(1)} fusion(f32[1,512,20,128]{1,3,2,0:T(8,128)S(1)} %bitcast.407, f32[2560,512,1]{1,0,2:T(8,128)S(1)} %bitcast.413, f32[512,20]{0,1:T(8,128)S(1)} %slice_bitcast_fusion.41, s32[512]{0:T(512)S(1)} %iota_add_fusion.1), kind=kLoop, calls=%fused_computation.36 | loop fusion | flops 28835840 | bytes 13150208 | tf_op jit(solution)/shard_map/convert_element_type | solution.py:91
  295.2 10.9 %fusion.4 = bf16[1,512,3072]{1,2,0:T(8,128)(2,1)S(1)} fusion(f32[1,512,24,128]{1,3,2,0:T(8,128)S(1)} %bitcast.405, f32[3072,512]{1,0:T(8,128)S(1)} %bitcast.409, f32[512,24]{0,1:T(8,128)S(1)} %slice_bitcast_fusion.39, f32[3072]{0:T(1024)S(1)} %bitcast.433, s32[512]{0:T(512)S(1)} %iota_add_fusion), kind=kLoop, calls=%fused_computation.12 | loop fusion | flops 37748736 | bytes 15792128 | tf_op jit(solution)/shard_map/convert_element_type | solution.py:91
  311.4 12.0 %all_to_all.45 = bf16[16,2,6144]{2,1,0:T(2,128)(2,1)S(1)} all-to-all(bf16[16,2,6144]{2,1,0:T(2,128)(2,1)S(1)} %reshape.793), channel_id=1, replica_groups=mesh['sp'=16,'dp'=8] {'sp'}, dimensions={0} | all-to-all | bytes 786432 | tf_op jit(solution)/shard_map/all_to_all | solution.py:101
  326.5 4.1 %fusion.59 = bf16[1,192,2048]{2,1,0:T(8,128)(2,1)} fusion(bf16[192,1024]{0,1:T(8,128)(2,1)S(1)} %bitcast.423, bf16[1024,2048]{1,0:T(8,128)(2,1)} %all-gather.5.cloned.1.call-done), kind=kOutput, calls=%fused_computation.93 | convolution fusion | flops 805699584 | bytes 5373952 | tf_op jit(solution)/shard_map/dot_general | solution.py:103
  (119 shorter events, 22.5 us)
Async XLA Ops:
  6.5 103.5 %all-gather.3.cloned.1.call-start = ((), (), s32[]{:S(2)}) async-start(), calls=%async_computation.3 | async-start | bytes 2228224 | tf_op jit(solution)/shard_map/all_gather | solution.py:22
  22.9 2.0 copy-start.3
  24.9 8.2 %copy-start.5 = (bf16[1,192,2048]{2,1,0:T(8,128)(2,1)S(1)}, bf16[1,192,2048]{2,1,0:T(8,128)(2,1)}, u32[]{:S(2)}) copy-start(bf16[1,192,2048]{2,1,0:T(8,128)(2,1)} %param.8) | copy-start | bytes 2359300
  24.9 85.2 %copy-start.7 = (f32[2048]{0:T(1024)S(1)}, f32[2048]{0:T(1024)}, u32[]{:S(2)}) copy-start(f32[2048]{0:T(1024)} %param.9) | copy-start | bytes 24580
  24.9 88.9 %all-to-all-start = ((bf16[2048,16,64]{0,2,1:T(8,128)(2,1)}), bf16[2048,16,64]{0,2,1:T(8,128)(2,1)}, u32[]{:S(2)}, u32[]{:S(2)}) async-start(bf16[2048,16,64]{0,2,1:T(8,128)(2,1)} %bitcast.415), calls=%async_computation | async-start | bytes 8388608 | tf_op jit(solution)/shard_map/all_to_all | solution.py:13
  117.6 7.5 %copy-start.6 = (f32[1,3072,1]{1,2,0:T(1,128)S(1)}, f32[1,3072,1]{1,2,0:T(1,128)}, u32[]{:S(2)}) copy-start(f32[1,3072,1]{1,2,0:T(1,128)} %param.13) | copy-start | bytes 36868
  119.3 28.9 %all-to-all-start.1 = ((bf16[192,16,192]{0,2,1:T(8,128)(2,1)}), bf16[192,16,192]{0,2,1:T(8,128)(2,1)S(1)}, u32[]{:S(2)}, u32[]{:S(2)}) async-start(bf16[192,16,192]{0,2,1:T(8,128)(2,1)} %pad_maximum_fusion), calls=%async_computation.1 | async-start | bytes 3145728 | tf_op jit(solution)/shard_map/all_to_all | solution.py:38
  124.3 202.2 %all-gather.5.cloned.1.call-start = ((), (), s32[]{:S(2)}) async-start(), calls=%async_computation.4 | async-start | bytes 4456448 | tf_op jit(solution)/shard_map/all_gather | solution.py:105
  150.8 18.6 %copy-start.1 = (bf16[3072,1,192]{0,2,1:T(8,128)(2,1)}, bf16[3072,1,192]{0,2,1:T(8,128)(2,1)S(1)}, u32[]{:S(2)}) copy-start(bf16[3072,1,192]{0,2,1:T(8,128)(2,1)S(1)} %all_to_all.38) | copy-start | bytes 3538948
  264.4 8.5 %copy-start.4 = (f32[1,512,1536]{1,2,0:T(8,128)S(1)}, f32[1,512,1536]{1,2,0:T(8,128)}, u32[]{:S(2)}) copy-start(f32[1,512,1536]{1,2,0:T(8,128)} %get-tuple-element.14) | copy-start | bytes 9437188
  264.5 22.4 %slice-start.6 = ((s8[5242880]{0:T(1024)(128)(4,1)}), s8[4194304]{0:T(1024)(128)(4,1)S(1)}, s32[]{:S(2)}) async-start(s8[5242880]{0:T(1024)(128)(4,1)} %bitcast.412), calls=%async_computation.11 | async-start | bytes 8388608
  267.1 19.8 %slice-start.2 = ((s8[5242880]{0:T(1024)(128)(4,1)}), s8[4194304]{0:T(1024)(128)(4,1)S(1)}, s32[]{:S(2)}) async-start(s8[5242880]{0:T(1024)(128)(4,1)} %bitcast.406), calls=%async_computation.7 | async-start | bytes 8388608
  272.9 5.0 %copy-start = (f32[1,512,16,128]{1,3,2,0:T(8,128)S(1)}, f32[1,512,16,128]{1,3,2,0:T(8,128)}, u32[]{:S(2)}) copy-start(f32[1,512,16,128]{1,3,2,0:T(8,128)} %copy.67) | copy-start | bytes 12582916
  272.9 14.0 %slice-start.3 = ((s8[5242880]{0:T(1024)(128)(4,1)}), s8[1048576]{0:T(1024)(128)(4,1)S(1)}, s32[]{:S(2)}) async-start(s8[5242880]{0:T(1024)(128)(4,1)} %bitcast.406), calls=%async_computation.8 | async-start | bytes 2097152
  272.9 14.0 %slice-start.7 = ((s8[5242880]{0:T(1024)(128)(4,1)}), s8[1048576]{0:T(1024)(128)(4,1)S(1)}, s32[]{:S(2)}) async-start(s8[5242880]{0:T(1024)(128)(4,1)} %bitcast.412), calls=%async_computation.12 | async-start | bytes 2097152
  277.9 17.2 %slice-start = ((s8[6291456]{0:T(1024)(128)(4,1)}), s8[4194304]{0:T(1024)(128)(4,1)S(1)}, s32[]{:S(2)}) async-start(s8[6291456]{0:T(1024)(128)(4,1)} %bitcast.404), calls=%async_computation.5 | async-start | bytes 8388608
  277.9 17.2 %slice-start.4 = ((s8[6291456]{0:T(1024)(128)(4,1)}), s8[2097152]{0:T(1024)(128)(4,1)S(1)}, s32[]{:S(2)}) async-start(s8[6291456]{0:T(1024)(128)(4,1)} %bitcast.408), calls=%async_computation.9 | async-start | bytes 4194304
  286.9 8.2 %slice-start.1 = ((s8[6291456]{0:T(1024)(128)(4,1)}), s8[2097152]{0:T(1024)(128)(4,1)S(1)}, s32[]{:S(2)}) async-start(s8[6291456]{0:T(1024)(128)(4,1)} %bitcast.404), calls=%async_computation.6 | async-start | bytes 4194304
  286.9 8.2 %slice-start.5 = ((s8[6291456]{0:T(1024)(128)(4,1)}), s8[4194304]{0:T(1024)(128)(4,1)S(1)}, s32[]{:S(2)}) async-start(s8[6291456]{0:T(1024)(128)(4,1)} %bitcast.408), calls=%async_computation.10 | async-start | bytes 8388608
  295.2 10.9 %copy-start.2 = (bf16[3072,1,192]{0,2,1:T(8,128)(2,1)S(1)}, bf16[3072,1,192]{0,2,1:T(8,128)(2,1)}, u32[]{:S(2)}) copy-start(bf16[3072,1,192]{0,2,1:T(8,128)(2,1)} %copy-done.1) | copy-start | bytes 3538948
Sparse Core Ops, SparseCore 0:
  21.9 88.1 all-gather.2
  127.2 53.8 all-gather.4
